TPU v7x, 32 devices: a whole 2x2x4 slice. The times are simulated.
32 devices in a mesh: sp: 4 (over y, x), tp: 8 (over z, core).
Axes of the slice: x: 2, y: 2, z: 4, core: 2. Of those that a mesh axis runs over, the one named last changes fastest.
Arguments:
- target: bfloat16 [512, 2048], P('sp'), may hold values from -6 to 6
- source: bfloat16 [1536, 2048], P('sp'), may hold values from -6 to 6
- cotangent: bfloat16 [512, 2048], P('sp'), may hold values from -192 to 192
- target_gain: float32 [2048], replicated, may hold values from 0.1 to 1.9
- source_gain: float32 [2048], replicated, may hold values from 0.1 to 1.9
- w_query: bfloat16 [2048, 4096], P(None, 'tp'), may hold values from -0.125 to 0.125
- w_key: bfloat16 [2048, 128], replicated, may hold values from -0.125 to 0.125
- w_value: bfloat16 [2048, 128], replicated, may hold values from -0.125 to 0.125
- w_out: bfloat16 [4096, 2048], P('tp'), may hold values from -0.09375 to 0.09375
Outputs:
- grad_target: bfloat16 [512, 2048], P(('sp', 'tp'))
- grad_source: bfloat16 [1536, 2048], P(('sp', 'tp'))
- grad_out_w: bfloat16 [4096, 2048], P('tp', 'sp')
All inputs are finite; a program needn't handle non-finite values.
Results may differ from a plain program's by a relative error of at most 0.025.
Values may be sent and summed in bfloat16 or wider, within the bound.
A program may use at most 64 MiB of HBM per device.

v0:
```python
import jax
import jax.numpy as jnp
from jax import lax
from jax.sharding import PartitionSpec as P

HEAD = 128


NORM_EPS = 1e-06
KEY_BLOCK = 1024
QUERY_BLOCK = 256


def normed(row_block, gain_vec):
    rows_wide = row_block.astype(jnp.float32)
    inv_rms = lax.rsqrt(jnp.mean(rows_wide * rows_wide, axis=1, keepdims=True) + NORM_EPS)
    return (rows_wide * inv_rms * gain_vec).astype(jnp.bfloat16)


def norm_back(row_block, gain_vec, upstream):
    rows_wide = row_block.astype(jnp.float32)
    inv_rms = lax.rsqrt(jnp.mean(rows_wide * rows_wide, axis=1, keepdims=True) + NORM_EPS)
    unit_rows = rows_wide * inv_rms
    pulled = upstream * gain_vec
    return inv_rms * (pulled - unit_rows * jnp.mean(pulled * unit_rows, axis=1, keepdims=True))


def block_span(row_count, largest):
    if row_count > largest and row_count % largest == 0:
        return largest
    return row_count


def right_product(left_rows, weight_mat):
    return lax.dot_general(
        left_rows, weight_mat, (((1,), (1,)), ((), ())), preferred_element_type=jnp.float32
    )


def on_device(target, source, cotangent, target_gain, source_gain, w_query, w_key, w_value, w_out):
    tp_count = lax.axis_size("tp")
    tp_place = lax.axis_index("tp")
    group_rows = target.shape[0]
    q_width = w_query.shape[1]
    heads_here = q_width // HEAD
    inv_root = HEAD ** (-0.5)
    query_all = jnp.dot(
        normed(target, target_gain), w_query, preferred_element_type=jnp.float32
    ).astype(jnp.bfloat16)
    grad_all = right_product(cotangent, w_out).astype(jnp.bfloat16)
    cot_columns = lax.all_to_all(cotangent, "sp", split_axis=1, concat_axis=0, tiled=True)
    source_rows = source.shape[0] // tp_count
    source_part = lax.dynamic_slice_in_dim(source, tp_place * source_rows, source_rows, 0)
    source_normed = normed(source_part, source_gain)
    key_own = jnp.dot(source_normed, w_key, preferred_element_type=jnp.float32).astype(jnp.bfloat16)
    value_own = jnp.dot(source_normed, w_value, preferred_element_type=jnp.float32).astype(
        jnp.bfloat16
    )
    key_group, value_group = (
        lax.all_gather(key_own, "tp", axis=0, tiled=True),
        lax.all_gather(value_own, "tp", axis=0, tiled=True),
    )
    query_heads = query_all.reshape(group_rows, heads_here, HEAD)
    grad_heads = grad_all.reshape(group_rows, heads_here, HEAD)
    empty_stat = jnp.zeros((group_rows, heads_here), jnp.float32)
    empty_acc = jnp.zeros((group_rows, heads_here, HEAD), jnp.float32)
    start_state = (empty_stat, empty_acc, empty_acc, empty_acc)
    key_piece = lax.all_gather(key_group, "sp", axis=0, tiled=True)
    value_piece = lax.all_gather(value_group, "sp", axis=0, tiled=True)
    piece_rows = key_piece.shape[0]
    step_rows = block_span(piece_rows, KEY_BLOCK)

    def attend_one_block(block_index, loop_state):
        row_total, output_sum, tilted_sum, weight_sum = loop_state
        key_block = lax.dynamic_slice_in_dim(key_piece, block_index * step_rows, step_rows, 0)
        value_block = lax.dynamic_slice_in_dim(value_piece, block_index * step_rows, step_rows, 0)
        scores = (
            jnp.einsum("ihd,jd->ihj", query_heads, key_block, preferred_element_type=jnp.float32)
            * inv_root
        )
        exponent = jnp.exp(scores)
        weights = exponent.astype(jnp.bfloat16)
        prob_grad = jnp.einsum(
            "ihd,jd->ihj", grad_heads, value_block, preferred_element_type=jnp.float32
        )
        tilted = (exponent * prob_grad).astype(jnp.bfloat16)
        row_total = row_total + jnp.sum(exponent, axis=2)
        output_sum = output_sum + jnp.einsum(
            "ihj,jd->ihd", weights, value_block, preferred_element_type=jnp.float32
        )
        tilted_sum = tilted_sum + jnp.einsum(
            "ihj,jd->ihd", tilted, key_block, preferred_element_type=jnp.float32
        )
        weight_sum = weight_sum + jnp.einsum(
            "ihj,jd->ihd", weights, key_block, preferred_element_type=jnp.float32
        )
        return (row_total, output_sum, tilted_sum, weight_sum)

    row_total, output_sum, tilted_sum, weight_sum = lax.fori_loop(
        0, piece_rows // step_rows, attend_one_block, start_state
    )
    attended = (output_sum / row_total[:, :, None]).astype(jnp.bfloat16)
    delta_row = jnp.sum(attended.astype(jnp.float32) * grad_heads.astype(jnp.float32), axis=2)
    grad_query = (
        (tilted_sum - delta_row[:, :, None] * weight_sum) / row_total[:, :, None] * inv_root
    ).astype(jnp.bfloat16)
    all_total, all_delta = (
        lax.all_gather(row_total, "sp", axis=0, tiled=True),
        lax.all_gather(delta_row, "sp", axis=0, tiled=True),
    )
    empty_keys = jnp.zeros((key_group.shape[0], HEAD), jnp.float32)
    query_piece = lax.all_gather(query_all, "sp", axis=0, tiled=True)
    grad_piece = lax.all_gather(grad_all, "sp", axis=0, tiled=True)
    piece_rows = query_piece.shape[0]
    collect_step_rows = block_span(piece_rows, QUERY_BLOCK)

    def collect_one_block(block_index, loop_state):
        key_grad, value_grad = loop_state
        local_begin = block_index * collect_step_rows
        query_block = lax.dynamic_slice_in_dim(
            query_piece, local_begin, collect_step_rows, 0
        ).reshape(collect_step_rows, heads_here, HEAD)
        grad_block = lax.dynamic_slice_in_dim(
            grad_piece, local_begin, collect_step_rows, 0
        ).reshape(collect_step_rows, heads_here, HEAD)
        total_block = lax.dynamic_slice_in_dim(all_total, local_begin, collect_step_rows, 0)
        delta_block = lax.dynamic_slice_in_dim(all_delta, local_begin, collect_step_rows, 0)
        scores = (
            jnp.einsum("ihd,jd->ihj", query_block, key_group, preferred_element_type=jnp.float32)
            * inv_root
        )
        prob_rows = jnp.exp(scores) / total_block[:, :, None]
        prob_grad = jnp.einsum(
            "ihd,jd->ihj", grad_block, value_group, preferred_element_type=jnp.float32
        )
        score_grad = (prob_rows * (prob_grad - delta_block[:, :, None])).astype(jnp.bfloat16)
        key_grad = (
            key_grad
            + jnp.einsum("ihj,ihd->jd", score_grad, query_block, preferred_element_type=jnp.float32)
            * inv_root
        )
        value_grad = value_grad + jnp.einsum(
            "ihj,ihd->jd",
            prob_rows.astype(jnp.bfloat16),
            grad_block,
            preferred_element_type=jnp.float32,
        )
        return (key_grad, value_grad)

    key_grad, value_grad = lax.fori_loop(
        0, piece_rows // collect_step_rows, collect_one_block, (empty_keys, empty_keys)
    )
    key_sum, value_sum = (
        lax.psum_scatter(
            key_grad.astype(jnp.bfloat16), "tp", scatter_dimension=0, tiled=True
        ).astype(jnp.float32),
        lax.psum_scatter(
            value_grad.astype(jnp.bfloat16), "tp", scatter_dimension=0, tiled=True
        ).astype(jnp.float32),
    )
    pulled_source = right_product(key_sum.astype(jnp.bfloat16), w_key) + right_product(
        value_sum.astype(jnp.bfloat16), w_value
    )
    grad_source = norm_back(source_part, source_gain, pulled_source).astype(jnp.bfloat16)
    query_grad_rows = grad_query.reshape(group_rows, q_width)
    target_rows = group_rows // tp_count
    pulled_target = lax.psum_scatter(
        right_product(query_grad_rows, w_query).astype(jnp.bfloat16),
        "tp",
        scatter_dimension=0,
        tiled=True,
    ).astype(jnp.float32)
    target_part = lax.dynamic_slice_in_dim(target, tp_place * target_rows, target_rows, 0)
    grad_target = norm_back(target_part, target_gain, pulled_target).astype(jnp.bfloat16)
    attended_rows = attended.reshape(group_rows, q_width)
    grad_out = lax.dot_general(
        lax.all_gather(attended_rows, "sp", axis=0, tiled=True),
        cot_columns,
        (((0,), (0,)), ((), ())),
        preferred_element_type=jnp.float32,
    )
    return (grad_target, grad_source, grad_out.astype(jnp.bfloat16))


def solution(mesh):
    in_specs = (
        P("sp", None),
        P("sp", None),
        P("sp", None),
        P(),
        P(),
        P(None, "tp"),
        P(),
        P(),
        P("tp", None),
    )
    out_specs = (P(("sp", "tp"), None), P(("sp", "tp"), None), P("tp", "sp"))
    return jax.shard_map(
        on_device, mesh=mesh, in_specs=in_specs, out_specs=out_specs, check_vma=False
    )
```

profile of v0, /device:TPU:0, one launch (start us, length us, event | category | flops | bytes accessed | tf_op | source)
XLA Modules:
  0.0 221.8 jit_solution(9454115933237955824)
XLA Ops:
  7.3 2.7 %convolution_convert_fusion.2 = bf16[128,512]{1,0:T(8,128)(2,1)S(1)} fusion(bf16[128,2048]{1,0:T(8,128)(2,1)} %param.13, bf16[512,2048]{1,0:T(8,128)(2,1)} %param.19), kind=kOutput, calls=%fused_computation.33 | convolution fusion | flops 268500992 | bytes 2752512 | tf_op jit(solution)/shard_map/dot_general | solution.py:35
  10.1 12.3 %all_gather.33 = bf16[512,512]{1,0:T(8,128)(2,1)} all-gather(bf16[128,512]{1,0:T(8,128)(2,1)S(1)} %convolution_convert_fusion.2), channel_id=1, replica_groups=mesh['sp'=4,'tp'=8] {'sp'}, dimensions={0}, use_global_device_ids=true | all-gather | bytes 655360 | tf_op jit(solution)/shard_map/all_gather | solution.py:113
  24.8 14.1 %all_gather.27 = bf16[384,128]{1,0:T(8,128)(2,1)S(1)} all-gather(bf16[48,128]{1,0:T(8,128)(2,1)S(1)} %convolution_convert_fusion.5), channel_id=1, replica_groups=mesh['sp'=4,'tp'=8] {'tp'}, dimensions={0}, use_global_device_ids=true | all-gather | bytes 110592 | tf_op jit(solution)/shard_map/all_gather | solution.py:60
  38.9 9.4 %all_gather.28 = bf16[1536,128]{1,0:T(8,128)(2,1)S(1)} all-gather(bf16[384,128]{1,0:T(8,128)(2,1)S(1)} %all_gather.27), channel_id=1, replica_groups=mesh['sp'=4,'tp'=8] {'sp'}, dimensions={0}, use_global_device_ids=true | all-gather | bytes 491520 | tf_op jit(solution)/shard_map/all_gather | solution.py:68
  49.0 10.1 %all_gather.31 = bf16[512,512]{1,0:T(8,128)(2,1)} all-gather(bf16[128,512]{1,0:T(8,128)(2,1)S(1)} %convolution_convert_fusion.3), channel_id=1, replica_groups=mesh['sp'=4,'tp'=8] {'sp'}, dimensions={0}, use_global_device_ids=true | all-gather | bytes 655360 | tf_op jit(solution)/shard_map/all_gather | solution.py:112
  61.6 13.9 %all_gather.29 = bf16[384,128]{1,0:T(8,128)(2,1)S(1)} all-gather(bf16[48,128]{1,0:T(8,128)(2,1)S(1)} %convolution_convert_fusion.4), channel_id=1, replica_groups=mesh['sp'=4,'tp'=8] {'tp'}, dimensions={0}, use_global_device_ids=true | all-gather | bytes 110592 | tf_op jit(solution)/shard_map/all_gather | solution.py:61
  75.5 9.8 %all_gather.30 = bf16[1536,128]{1,0:T(8,128)(2,1)S(1)} all-gather(bf16[384,128]{1,0:T(8,128)(2,1)S(1)} %all_gather.29), channel_id=1, replica_groups=mesh['sp'=4,'tp'=8] {'sp'}, dimensions={0}, use_global_device_ids=true | all-gather | bytes 491520 | tf_op jit(solution)/shard_map/all_gather | solution.py:69
  85.3 6.8 %all_gather.32 = f32[512,4]{0,1:T(4,128)S(1)} all-gather(f32[128,4]{0,1:T(4,128)S(1)} %get-tuple-element.260), channel_id=1, replica_groups=mesh['sp'=4,'tp'=8] {'sp'}, dimensions={0}, use_global_device_ids=true | all-gather | bytes 10240 | tf_op jit(solution)/shard_map/all_gather | solution.py:108
  93.4 8.4 %all_gather.34 = f32[512,4]{0,1:T(4,128)S(1)} all-gather(f32[128,4]{0,1:T(4,128)S(1)} %get-tuple-element.262), channel_id=1, replica_groups=mesh['sp'=4,'tp'=8] {'sp'}, dimensions={0}, use_global_device_ids=true | all-gather | bytes 10240 | tf_op jit(solution)/shard_map/all_gather | solution.py:109
  101.8 16.5 %while.10 = (s32[]{:T(128)}, f32[384,128]{1,0:T(8,128)S(1)}, f32[384,128]{1,0:T(8,128)S(1)}, bf16[512,512]{1,0:T(8,128)(2,1)}, bf16[384,128]{1,0:T(8,128)(2,1)},...) while((s32[]{:T(128)}, f32[384,128]{1,0:T(8,128)S(1)}, ...), condition=%wide.region_8.0_spmd.clone, body=%wide.region_7.0_spmd.clone.sunk | while | flops 405258240 | bytes 8872134 | solution.py:150
  103.0 2.5 %exponential_divide_fusion.2 = f32[256,4,384]{2,0,1:T(8,128)} fusion(bf16[256,4,128]{0,2,1:T(8,128)(2,1)S(1)} %bitcast.95, f32[256,4]{0,1:T(4,128)S(1)} %get-tuple-element.326, bf16[384,128]{1,0:T(8,128)(2,1)} %get-tuple-element.359), kind=kOutput, calls=%fused_computation.1.clone.1 | convolution fusion | flops 101449728 | bytes 1937408 | tf_op jit(solution)/shard_map/while/body/eval_jaxpr/ihd,jd->ihj/dot_general | solution.py:129
  105.7 2.5 %fusion.92 = f32[384,128]{1,0:T(8,128)S(1)} fusion(bf16[256,4,128]{0,2,1:T(8,128)(2,1)S(1)} %bitcast.96, f32[256,4,384]{2,0,1:T(8,128)} %exponential_divide_fusion.2, bf16[256,4,128]{0,2,1:T(8,128)(2,1)S(1)} %bitcast.93, f32[256,4]{0,1:T(4,128)S(1)} %get-tuple-element.328, f32[384,128]{1,0:T(8,128)S(1)} %get-tuple-element.343, ...), kind=kOutput, calls=%fused_computation.6.clone.1 | convolution fusion | flops 202653696 | bytes 2592769 | tf_op jit(solution)/shard_map/while/body/eval_jaxpr/ihj,ihd->jd/dot_general | solution.py:139
  111.3 2.6 %exponential_divide_fusion.2 = f32[256,4,384]{2,0,1:T(8,128)} fusion(bf16[256,4,128]{0,2,1:T(8,128)(2,1)S(1)} %bitcast.95, f32[256,4]{0,1:T(4,128)S(1)} %get-tuple-element.326, bf16[384,128]{1,0:T(8,128)(2,1)} %get-tuple-element.359), kind=kOutput, calls=%fused_computation.1.clone.1 | convolution fusion | flops 101449728 | bytes 1937408 | tf_op jit(solution)/shard_map/while/body/eval_jaxpr/ihd,jd->ihj/dot_general | solution.py:129
  114.0 2.5 %fusion.92 = f32[384,128]{1,0:T(8,128)S(1)} fusion(bf16[256,4,128]{0,2,1:T(8,128)(2,1)S(1)} %bitcast.96, f32[256,4,384]{2,0,1:T(8,128)} %exponential_divide_fusion.2, bf16[256,4,128]{0,2,1:T(8,128)(2,1)S(1)} %bitcast.93, f32[256,4]{0,1:T(4,128)S(1)} %get-tuple-element.328, f32[384,128]{1,0:T(8,128)S(1)} %get-tuple-element.343, ...), kind=kOutput, calls=%fused_computation.6.clone.1 | convolution fusion | flops 202653696 | bytes 2592769 | tf_op jit(solution)/shard_map/while/body/eval_jaxpr/ihj,ihd->jd/dot_general | solution.py:139
  116.5 1.8 fusion.93
  119.0 2.0 copy.45
  121.1 4.1 %all-to-all-start = ((bf16[128,4,512]{0,2,1:T(8,128)(2,1)}), bf16[128,4,512]{0,2,1:T(8,128)(2,1)}, u32[]{:S(2)}, u32[]{:S(2)}) async-start(bf16[128,4,512]{0,2,1:T(8,128)(2,1)} %bitcast.7), calls=%async_computation.3 | async-start | bytes 1048576 | tf_op jit(solution)/shard_map/all_to_all | solution.py:51
  126.0 2.6 %convolution_multiply_fusion.2 = f32[128,4,128]{0,2,1:T(8,128)S(1)} fusion(f32[128,4,1536]{2,0,1:T(8,128)} %copy-done.1, bf16[1536,128]{1,0:T(8,128)(2,1)S(1)} %copy-done.3, f32[128,4]{0,1:T(4,128)S(1)} %get-tuple-element.262), kind=kOutput, calls=%fused_computation.28 | convolution fusion | flops 202178560 | bytes 3803136 | tf_op jit(solution)/shard_map/while/body/eval_jaxpr/ihj,jd->ihd/dot_general | solution.py:94
  128.6 3.6 %fusion.17 = bf16[128,4,128]{0,2,1:T(8,128)(2,1)} fusion(f32[128,4,128]{0,2,1:T(8,128)S(1)} %convolution_multiply_fusion.2, f32[128,4,1536]{2,0,1:T(8,128)} %copy-done.1, bf16[128,4,128]{0,2,1:T(8,128)(2,1)S(1)} %bitcast.98, bf16[1536,128]{1,0:T(8,128)(2,1)S(1)} %copy-done.5, bf16[1536,128]{1,0:T(8,128)(2,1)S(1)} %copy-done.3, ...), kind=kOutput, calls=%fused_computation.32 | convolution fusion | flops 404488192 | bytes 4458496 | tf_op jit(solution)/shard_map/while/body/eval_jaxpr/ihj,jd->ihd/dot_general | solution.py:91
  132.2 2.6 %convolution_convert_fusion = bf16[128,2048]{1,0:T(8,128)(2,1)} fusion(bf16[128,512]{0,1:T(8,128)(2,1)} %bitcast.100, bf16[2048,512]{1,0:T(8,128)(2,1)S(1)} %copy-done), kind=kOutput, calls=%fused_computation.20 | convolution fusion | flops 268697600 | bytes 2752512 | tf_op jit(solution)/shard_map/dot_general | solution.py:35
  136.4 10.5 %all_gather.35 = bf16[512,512]{0,1:T(8,128)(2,1)S(1)} all-gather(bf16[128,512]{0,1:T(8,128)(2,1)S(1)} %bitcast.99), channel_id=1, replica_groups=mesh['sp'=4,'tp'=8] {'sp'}, dimensions={0}, use_global_device_ids=true | all-gather | bytes 655360 | tf_op jit(solution)/shard_map/all_gather | solution.py:177
  146.9 2.9 %reduce-scatter.6.cloned.1.call-done = bf16[48,128]{1,0:T(8,128)(2,1)} async-done(((bf16[384,128]{1,0:T(8,128)(2,1)}), bf16[48,128]{1,0:T(8,128)(2,1)}) %reduce-scatter.6.cloned.1.call-update) | async-done | bytes 12304 | tf_op jit(solution)/shard_map/reduce_scatter | solution.py:154
  151.1 29.6 %reduce-scatter.8.cloned.1.call-done = bf16[48,128]{1,0:T(8,128)(2,1)} async-done(((bf16[384,128]{1,0:T(8,128)(2,1)}), bf16[48,128]{1,0:T(8,128)(2,1)}) %reduce-scatter.8.cloned.1.call-update) | async-done | bytes 12304 | tf_op jit(solution)/shard_map/reduce_scatter | solution.py:157
  186.4 26.2 %reduce-scatter.4.cloned.1.call-done = bf16[16,2048]{1,0:T(8,128)(2,1)} async-done(((bf16[128,2048]{1,0:T(8,128)(2,1)}), bf16[16,2048]{1,0:T(8,128)(2,1)}) %reduce-scatter.4.cloned.1.call-update) | async-done | bytes 65552 | tf_op jit(solution)/shard_map/reduce_scatter | solution.py:167
  (73 shorter events, 24.1 us)
Async XLA Ops:
  7.2 41.4 %copy-start = (bf16[2048,512]{1,0:T(8,128)(2,1)S(1)}, bf16[2048,512]{1,0:T(8,128)(2,1)}, u32[]{:S(2)}) copy-start(bf16[2048,512]{1,0:T(8,128)(2,1)} %param.16) | copy-start | bytes 6291460
  7.2 142.6 %reduce-scatter.6.cloned.1.call-start = ((), (), s32[]{:S(2)}) async-start(), calls=%async_computation.5 | async-start | bytes 110592 | tf_op jit(solution)/shard_map/reduce_scatter | solution.py:154
  7.2 16.3 %copy-start.8 = (bf16[2048,128]{1,0:T(8,128)(2,1)S(1)}, bf16[2048,128]{1,0:T(8,128)(2,1)}, u32[]{:S(2)}) copy-start(bf16[2048,128]{1,0:T(8,128)(2,1)} %param.17) | copy-start | bytes 1572868
  7.3 16.3 %copy-start.12 = (f32[2048]{0:T(1024)S(1)}, f32[2048]{0:T(1024)}, u32[]{:S(2)}) copy-start(f32[2048]{0:T(1024)} %param.15) | copy-start | bytes 24580
  10.0 38.5 %copy-start.13 = (f32[2048]{0:T(1024)S(1)}, f32[2048]{0:T(1024)}, u32[]{:S(2)}) copy-start(f32[2048]{0:T(1024)} %param.14) | copy-start | bytes 24580
  22.4 25.9 %copy-start.9 = (bf16[128,2048]{1,0:T(8,128)(2,1)S(1)}, bf16[128,2048]{1,0:T(8,128)(2,1)}, u32[]{:S(2)}) copy-start(bf16[128,2048]{1,0:T(8,128)(2,1)} %param.11) | copy-start | bytes 1572868
  23.6 36.3 %copy-start.14 = (f32[48]{0:T(128)}, f32[48]{0:T(128)S(1)}, u32[]{:S(2)}) copy-start(f32[48]{0:T(128)S(1)} %add_rsqrt_fusion) | copy-start | bytes 580
  38.9 9.6 %copy-start.11 = (bf16[384,128]{1,0:T(8,128)(2,1)}, bf16[384,128]{1,0:T(8,128)(2,1)S(1)}, u32[]{:S(2)}) copy-start(bf16[384,128]{1,0:T(8,128)(2,1)S(1)} %all_gather.27) | copy-start | bytes 294916
  48.3 10.8 %copy-start.2 = (bf16[1536,128]{1,0:T(8,128)(2,1)}, bf16[1536,128]{1,0:T(8,128)(2,1)S(1)}, u32[]{:S(2)}) copy-start(bf16[1536,128]{1,0:T(8,128)(2,1)S(1)} %all_gather.28) | copy-start | bytes 1179652
  59.1 1.0 copy-start.6
  60.2 33.3 %copy-start.1 = (f32[128,4,1536]{2,0,1:T(8,128)}, f32[128,4,1536]{2,0,1:T(8,128)S(1)}, u32[]{:S(2)}) copy-start(f32[128,4,1536]{2,0,1:T(8,128)S(1)} %get-tuple-element.261) | copy-start | bytes 9437188
  85.3 8.1 %copy-start.4 = (bf16[1536,128]{1,0:T(8,128)(2,1)}, bf16[1536,128]{1,0:T(8,128)(2,1)S(1)}, u32[]{:S(2)}) copy-start(bf16[1536,128]{1,0:T(8,128)(2,1)S(1)} %all_gather.30) | copy-start | bytes 1179652
  118.3 7.7 %copy-start.3 = (bf16[1536,128]{1,0:T(8,128)(2,1)S(1)}, bf16[1536,128]{1,0:T(8,128)(2,1)}, u32[]{:S(2)}) copy-start(bf16[1536,128]{1,0:T(8,128)(2,1)} %copy-done.2) | copy-start | bytes 1179652
  121.1 62.8 %all-to-all-start = ((bf16[128,4,512]{0,2,1:T(8,128)(2,1)}), bf16[128,4,512]{0,2,1:T(8,128)(2,1)}, u32[]{:S(2)}, u32[]{:S(2)}) async-start(bf16[128,4,512]{0,2,1:T(8,128)(2,1)} %bitcast.7), calls=%async_computation.3 | async-start | bytes 1048576 | tf_op jit(solution)/shard_map/all_to_all | solution.py:51
  125.2 55.6 %reduce-scatter.8.cloned.1.call-start = ((), (), s32[]{:S(2)}) async-start(), calls=%async_computation.6 | async-start | bytes 110592 | tf_op jit(solution)/shard_map/reduce_scatter | solution.py:157
  125.9 2.7 %copy-start.5 = (bf16[1536,128]{1,0:T(8,128)(2,1)S(1)}, bf16[1536,128]{1,0:T(8,128)(2,1)}, u32[]{:S(2)}) copy-start(bf16[1536,128]{1,0:T(8,128)(2,1)} %copy-done.4) | copy-start | bytes 1179652
  126.0 86.7 %reduce-scatter.4.cloned.1.call-start = ((), (), s32[]{:S(2)}) async-start(), calls=%async_computation.4 | async-start | bytes 589824 | tf_op jit(solution)/shard_map/reduce_scatter | solution.py:167
  132.2 4.1 %copy-start.10 = (bf16[128,4,128]{0,2,1:T(8,128)(2,1)S(1)}, bf16[128,4,128]{0,2,1:T(8,128)(2,1)}, u32[]{:S(2)}) copy-start(bf16[128,4,128]{0,2,1:T(8,128)(2,1)} %get-tuple-element.263) | copy-start | bytes 393220
  134.8 46.0 %copy-start.7 = (bf16[2048,128]{1,0:T(8,128)(2,1)S(1)}, bf16[2048,128]{1,0:T(8,128)(2,1)}, u32[]{:S(2)}) copy-start(bf16[2048,128]{1,0:T(8,128)(2,1)} %param.18) | copy-start | bytes 1572868
  182.1 30.5 %copy-start.15 = (f32[16]{0:T(128)S(1)}, f32[16]{0:T(128)}, u32[]{:S(2)}) copy-start(f32[16]{0:T(128)} %add_rsqrt_fusion.2) | copy-start | bytes 196
Sparse Core Ops, SparseCore 0:
  119.1 30.5 reduce-scatter.5
  152.0 28.7 reduce-scatter.7
  183.0 29.5 reduce-scatter.3
where the time goes:
time: 223 us; the launch traced here: 222 us
  blocking collectives  95.2 us (43%)
  waiting for transfers between devices  58.9 us (26%)
  matrix products  34.2 us (15%)
  between operations  14 us (6%)
  other arithmetic  8.6 us (4%)
  local copies, waits for them, and re-layouts  6.51 us (3%)
  starting transfers between devices  4.25 us (2%)
    reduce_scatter x1, waiting for transfers between devices, on_device(): lax.psum_scatter(value_grad.astype(jnp.bfloat16), 'tp', scatter_dimension...  29.6 us
    reduce_scatter x1, waiting for transfers between devices, on_device(): lax.psum_scatter(right_product(query_grad_rows, w_query).astype(jnp.bfloa...  26.2 us
    all_gather x1, blocking collectives, on_device(): lax.all_gather(key_own, 'tp', axis=0, tiled=True)  14.1 us
    all_gather x1, blocking collectives, on_device(): lax.all_gather(value_own, 'tp', axis=0, tiled=True)  13.9 us
    all_gather x1, blocking collectives, on_device(): grad_piece = lax.all_gather(grad_all, 'sp', axis=0, tiled=True)  12.3 us
    all_gather x1, blocking collectives, on_device(): lax.all_gather(attended_rows, 'sp', axis=0, tiled=True)  10.5 us
    all_gather x1, blocking collectives, on_device(): query_piece = lax.all_gather(query_all, 'sp', axis=0, tiled=True)  10.1 us
    all_gather x1, blocking collectives, on_device(): value_piece = lax.all_gather(value_group, 'sp', axis=0, tiled=True)  9.79 us
  transfers between devices with their start and end apart: 4, of which 3 were waited for; matrix products, arithmetic and copies ran while one was open for 9% of the time, Pallas kernels for 0%

commit v1 on v0

v1 whole, which is shorter than its diff:
```python
import functools
import math

import jax
import jax.numpy as jnp
from jax import lax
from jax.experimental import pallas as pl
from jax.experimental.pallas import tpu as pltpu
from jax.sharding import PartitionSpec as P

HEAD = 128
NORM_EPS = 1e-06
CORES = 2
F32 = jnp.float32
BF16 = jnp.bfloat16
MESH = pl.DeviceIdType.MESH
NN = (((1,), (0,)), ((), ()))
NT = (((1,), (1,)), ((), ()))
TN = (((0,), (0,)), ((), ()))


def dot(a, b, dims=NN):
    return lax.dot_general(a, b, dims, preferred_element_type=F32)


def inv_rms_of(wide):
    return lax.rsqrt(jnp.mean(wide * wide, axis=1, keepdims=True) + NORM_EPS)


def norm_into(src, gain, dst, block):
    def body(i, _):
        rows = pl.ds(pl.multiple_of(i * block, block), block)
        wide = src[rows, :].astype(F32)
        dst[rows, :] = (wide * inv_rms_of(wide) * gain[...]).astype(BF16)
        return 0

    lax.fori_loop(0, src.shape[0] // block, body, 0)


def norm_back(wide, gain, upstream):
    inv = inv_rms_of(wide)
    unit = wide * inv
    pulled = upstream * gain
    return inv * (pulled - unit * jnp.mean(pulled * unit, axis=1, keepdims=True))


def own_rows(ref, place, rows):
    if rows % 16 == 0:
        return ref[pl.ds(pl.multiple_of(place * rows, 16), rows), :].astype(F32)
    padded = -(-rows // 16) * 16
    line = lax.broadcasted_iota(jnp.int32, (padded, ref.shape[0]), 0) + place * rows
    column = lax.broadcasted_iota(jnp.int32, (padded, ref.shape[0]), 1)
    pick = jnp.where(line == column, 1.0, 0.0).astype(BF16)
    return dot(pick, ref[...])[:rows]


def kernel(
    S, T,
    target_h, source_h, cot_h, tgain, sgain, wq_h, wk_h, wv_h, wo_h,
    gt_ref, gs_ref, go_ref,
    target, source, cot, wq, wkv, wo, normed, kv, cotb, att, e_buf,
    kvg, kvg_in, red, red_in, red2, fin_in, pt, pt_in, ptr, ptr_in, stage,
    load_sem, send, recv,
):
    Z = T // CORES
    me, t = lax.axis_index("sp"), lax.axis_index("tp")
    c, z = lax.rem(t, CORES), lax.div(t, CORES)
    sibling = {"sp": me, "tp": z * CORES + (1 - c)}
    TR, D = target.shape
    SG = source.shape[0]
    QW = wq.shape[1]
    H = QW // HEAD
    half = SG // 2
    thalf = TR // 2
    W = D // S
    SR, RR = SG // T, TR // T
    inv_root = HEAD ** (-0.5)

    def sp_peer(d):
        return {"sp": lax.rem(me + d, S), "tp": t}

    def z_peer(d):
        return {"sp": me, "tp": lax.rem(z + d, Z) * CORES + c}

    sends = []

    def put(src, dst, lane, slot, who):
        copy = pltpu.make_async_remote_copy(
            src_ref=src, dst_ref=dst, send_sem=send.at[lane, slot], recv_sem=recv.at[lane, slot],
            device_id=who, device_id_type=MESH,
        )
        copy.start()
        sends.append(copy)
        return copy

    loads = []
    for i, (a, b) in enumerate(
        (
            (source_h, source), (wk_h, wkv.at[:, :HEAD]), (wv_h, wkv.at[:, HEAD:]),
            (target_h, target), (wq_h, wq), (cot_h, cot), (wo_h, wo),
        )
    ):
        copy = pltpu.make_async_copy(a, b, load_sem.at[i])
        copy.start()
        loads.append(copy)

    barrier = pltpu.get_barrier_semaphore()
    friends = [sibling] + [sp_peer(d) for d in range(1, S)] + [z_peer(d) for d in range(1, Z)]
    for who in friends:
        pl.semaphore_signal(barrier, inc=1, device_id=who, device_id_type=MESH)

    loads[0].wait()
    norm_into(source, sgain, normed, 32)
    loads[1].wait()
    loads[2].wait()
    kv_own = dot(normed[...], wkv[...]).astype(BF16)
    kv[0, 0] = kv_own[:half]
    kv[0, 1] = kv_own[half:]
    pl.semaphore_wait(barrier, len(friends))
    kv_put = [None] + [put(kv.at[0, c], kv.at[d, c], 0, d, sp_peer(d)) for d in range(1, S)]
    loads[5].wait()
    cot_put = [None]
    for d in range(1, S):
        columns = pl.ds(pl.multiple_of(lax.rem(me + d, S) * W, 128), W)
        rows = pl.ds(pl.multiple_of(c * thalf, thalf), thalf)
        cot_put.append(put(cot.at[rows, columns], cotb.at[d, c], 1, d, sp_peer(d)))

    loads[3].wait()
    norm_into(target, tgain, normed, 32)
    loads[4].wait()
    query = dot(normed[:TR, :], wq[...]).astype(BF16)
    loads[6].wait()
    grad = dot(cot[...], wo[...], NT).astype(BF16)
    q_rows = jnp.concatenate([query[:, h * HEAD:(h + 1) * HEAD] for h in range(H)], axis=0)
    g_rows = jnp.concatenate([grad[:, h * HEAD:(h + 1) * HEAD] for h in range(H)], axis=0)

    def pair(d):
        both = jnp.concatenate([kv[d,0],kv[d,1]],axis=0)
        return both[:, :HEAD], both[:, HEAD:]

    def exponents(d):
        k, v = pair(d)
        e = jnp.exp2(dot(k, q_rows, NT) * (inv_root * math.log2(math.e)))
        e_buf[d] = e
        return jnp.sum(e, axis=0, keepdims=True), dot(v, e.astype(BF16), TN)

    total, out_t = exponents(0)
    kv_fwd = [None]
    for d in range(1, S):
        kv_put[d].wait_recv()
        kv_fwd.append(put(kv.at[d, c], kv.at[d, c], 2, d, sibling))
    for d in range(1, S):
        kv_fwd[d].wait_recv()
        more, out_more = exponents(d)
        total, out_t = total + more, out_t + out_more
    inv_total = 1.0 / total
    att_t = (out_t * inv_total).astype(BF16)
    att[0] = att_t
    delta = jnp.sum(att_t.astype(F32) * g_rows.astype(F32).T, axis=0, keepdims=True)
    att_put = [None] + [put(att.at[0], att.at[d], 3, d, sp_peer(d)) for d in range(1, S)]

    def spread(d, grads):
        if SR % 8:
            stage[...] = grads
        for place in range(T):
            rows = slice(place * SR, (place + 1) * SR)
            block = stage[rows, :] if SR % 8 else grads[rows]
            kvg[place % CORES, d, place // CORES] = block.astype(BF16)

    def settle(d):
        kvg_put[d].wait_recv()
        red[d] = (kvg[c, d].astype(F32) + kvg_in[d].astype(F32)).astype(BF16)
        if d:
            return put(red.at[d], red_in.at[d], 5, d, sp_peer(S - d))

    kvg_put = {}
    red_put = {}
    gq_t = None
    order = list(range(1, S)) + [0]
    for step, d in enumerate(order):
        k, v = pair(d)
        p = e_buf[d] * inv_total
        score_grad = (p * (dot(v, g_rows, NT) - delta)).astype(BF16)
        part = dot(k, score_grad, TN)
        gq_t = part if gq_t is None else gq_t + part
        k_grad = dot(score_grad, q_rows) * inv_root
        v_grad = dot(p.astype(BF16), g_rows)
        spread(d, jnp.concatenate([k_grad, v_grad], axis=1))
        kvg_put[d] = put(kvg.at[1 - c, d], kvg_in.at[d], 4, d, sibling)
        if step:
            red_put[order[step - 1]] = settle(order[step - 1])

    gq_t = gq_t * inv_root
    gq = jnp.concatenate([gq_t[:, h * TR:(h + 1) * TR].T for h in range(H)], axis=1).astype(BF16)
    pulled = dot(gq, wq[...], NT)
    for place in range(T):
        if RR % 8:
            if place == 0:
                normed_rows = stage_rows(e_buf, pulled)
            block = normed_rows(place * RR, RR)
        else:
            block = pulled[place * RR:(place + 1) * RR]
        pt[place % CORES, place // CORES] = block.astype(BF16)
    pt_put = put(pt.at[1 - c], pt_in, 6, 0, sibling)
    settle(0)
    cot_fwd = [None]
    for d in range(1, S):
        cot_put[d].wait_recv()
        cot_fwd.append(put(cotb.at[d, c], cotb.at[d, c], 7, d, sibling))
    pt_put.wait_recv()
    ptr[...] = (pt[c].astype(F32) + pt_in[...].astype(F32)).astype(BF16)
    ptr_put = [None] + [
        put(ptr.at[lax.rem(z + d, Z)], ptr_in.at[d], 8, d, z_peer(d)) for d in range(1, Z)
    ]
    summed = red[0].astype(F32)
    for d in range(1, S):
        red_put[d].wait_recv()
        summed = summed + red_in[d].astype(F32)
    red2[...] = summed.astype(BF16)
    fin_put = [None] + [
        put(red2.at[lax.rem(z + d, Z)], fin_in.at[d], 9, d, z_peer(d)) for d in range(1, Z)
    ]

    att_all, cot_all = [att[0]], [cot[:, pl.ds(pl.multiple_of(me * W, 128), W)]]
    for d in range(1, S):
        att_put[d].wait_recv()
        cot_fwd[d].wait_recv()
        att_all.append(att[d])
        cot_all.append(jnp.concatenate([cotb[d,0],cotb[d,1]],axis=0))
    cot_rows = jnp.concatenate(cot_all, axis=0)
    for h in range(H):
        left = jnp.concatenate([a[:, h * TR:(h + 1) * TR] for a in att_all], axis=1)
        go_ref[h * HEAD:(h + 1) * HEAD, :] = dot(left, cot_rows).astype(BF16)

    up = ptr[z].astype(F32)
    for d in range(1, Z):
        ptr_put[d].wait_recv()
        up = up + ptr_in[d].astype(F32)
    gt_ref[...] = norm_back(own_rows(target, t, RR), tgain[...], up).astype(BF16)
    last = red2[z].astype(F32)
    for d in range(1, Z):
        fin_put[d].wait_recv()
        last = last + fin_in[d].astype(F32)
    up = dot(last.astype(BF16), wkv[...], NT)
    gs_ref[...] = norm_back(own_rows(source, t, SR), sgain[...], up).astype(BF16)
    for copy in sends:
        copy.wait_send()


def stage_rows(buf, rows):
    width = buf.shape[2]
    bands = rows.shape[1] // width
    for i in range(bands):
        buf[i, :rows.shape[0], :] = rows[:, i * width:(i + 1) * width]
    return lambda start, count: jnp.concatenate(
        [buf[i, start:start + count, :] for i in range(bands)], axis=1
    )


def on_device(S, T, target, source, cotangent, target_gain, source_gain, w_query, w_key, w_value, w_out):
    TR, D = target.shape
    SG = source.shape[0]
    QW = w_query.shape[1]
    R = QW // HEAD * TR
    Z = T // CORES
    SR, RR, W = SG // T, TR // T, D // S
    N = max(S, Z)
    hbm = pl.BlockSpec(memory_space=pl.ANY)
    vm = pl.BlockSpec(memory_space=pltpu.VMEM)
    V = pltpu.VMEM
    return pl.pallas_call(
        functools.partial(kernel, S, T),
        out_shape=(
            jax.ShapeDtypeStruct((RR, D), BF16),
            jax.ShapeDtypeStruct((SR, D), BF16),
            jax.ShapeDtypeStruct((QW, W), BF16),
        ),
        in_specs=[hbm, hbm, hbm, vm, vm, hbm, hbm, hbm, hbm],
        out_specs=(vm, vm, vm),
        scratch_shapes=[
            V((TR, D), BF16), V((SG, D), BF16), V((TR, D), BF16),
            V((D, QW), BF16), V((D, 2 * HEAD), BF16), V((QW, D), BF16),
            V((max(SG, TR), D), BF16),
            V((S, 2, SG // 2, 2 * HEAD), BF16), V((S, 2, TR // 2, W), BF16),
            V((S, HEAD, R), BF16), V((S, SG, R), F32),
            V((CORES, S, Z, SR, 2 * HEAD), BF16), V((S, Z, SR, 2 * HEAD), BF16),
            V((S, Z, SR, 2 * HEAD), BF16), V((S, Z, SR, 2 * HEAD), BF16),
            V((Z, SR, 2 * HEAD), BF16), V((Z, SR, 2 * HEAD), BF16),
            V((CORES, Z, RR, D), BF16), V((Z, RR, D), BF16), V((Z, RR, D), BF16), V((Z, RR, D), BF16),
            V((SG, 2 * HEAD), F32),
            pltpu.SemaphoreType.DMA((7,)),
            pltpu.SemaphoreType.DMA((10, N)),
            pltpu.SemaphoreType.DMA((10, N)),
        ],
        compiler_params=pltpu.CompilerParams(
            collective_id=0, has_side_effects=True, vmem_limit_bytes=60 * 1024 * 1024
        ),
        name="attn_back",
    )(
        target, source, cotangent, target_gain.reshape(1, D), source_gain.reshape(1, D),
        w_query, w_key, w_value, w_out,
    )


def solution(mesh):
    in_specs = (
        P("sp", None), P("sp", None), P("sp", None), P(), P(),
        P(None, "tp"), P(), P(), P("tp", None),
    )
    out_specs = (P(("sp", "tp"), None), P(("sp", "tp"), None), P("tp", "sp"))
    return jax.shard_map(
        functools.partial(on_device, mesh.shape["sp"], mesh.shape["tp"]),
        mesh=mesh, in_specs=in_specs, out_specs=out_specs, check_vma=False,
    )
```

time: 223 us -> 41.1 us (0.18)
  blocking collectives: 95.2 us -> 0 us
  waiting for transfers between devices: 58.9 us -> 0 us
  Pallas kernels: 0 us -> 35.2 us
  matrix products: 34.2 us -> 0 us
  between operations: 14 us -> 0.64 us
  other arithmetic: 8.6 us -> 0 us
  starting transfers between devices: 4.25 us -> 0 us
    all_gather x9 -> x0, blocking collectives: 95.2 us -> none  [the longest x1 14.1 us: on_device(): lax.all_gather(key_own, 'tp', axis=0, tiled=True)]
    reduce_scatter x3 -> x0, waiting for transfers between devices: 58.8 us -> none  [the longest x1 29.6 us: on_device(): lax.psum_scatter(value_grad.astype(jnp.bfloat16), 'tp', scatter_dimension...]
    pallas_call x0 -> x1, Pallas kernels: none -> 35.2 us  [on_device(): pl.pallas_call(functools.partial(kernel, S, T), out_shape=(jax.ShapeDtype...]
    dot_general x18 -> x0, matrix products: 34.2 us -> none  [the longest x4 7.97 us: right_product(): lax.dot_general(left_rows, weight_mat, (((1,), (1,)), ((), ())), preferre...]
    convert_element_type x4 -> x0, other arithmetic: 4.64 us -> none  [the longest x1 1.75 us: on_device(): norm_back(source_part, source_gain, pulled_source).astype(jnp.bfloat16)]
    all_to_all x1 -> x0, starting transfers between devices: 4.13 us -> none  [on_device(): lax.all_to_all(cotangent, 'sp', split_axis=1, concat_axis=0, tiled=True)]
    reduce_sum x4 -> x0, other arithmetic: 3.41 us -> none  [the longest x2 1.32 us: normed(): jnp.mean(rows_wide * rows_wide, axis=1, keepdims=True) + NORM_EPS]
    dynamic_slice x8 -> x0, local copies, waits for them, and re-layouts: 2.69 us -> none  [the longest x4 2.4 us: collect_one_block(): lax.dynamic_slice_in_dim(grad_piece, local_begin, collect_step_rows, 0)]
  transfers between devices with their start and end apart: 4 -> 0, of which waited for: 3 -> 0; matrix products, arithmetic and copies ran while one was open for 9% -> 0% of each run, Pallas kernels for 0% -> 0%
where the time goes in v1:
time: 41.1 us; the launch traced here: 40.8 us
  Pallas kernels  35.2 us (86%)
  local copies, waits for them, and re-layouts  4.96 us (12%)
  between operations  0.64 us (2%)
    pallas_call x1, Pallas kernels, on_device(): pl.pallas_call(functools.partial(kernel, S, T), out_shape=(jax.ShapeDtype...  35.2 us
    unnamed x3, local copies, waits for them, and re-layouts  4.96 us

profile of v1, /device:TPU:0, one launch (start us, length us, event | category | flops | bytes accessed | tf_op | source)
XLA Modules:
  0.0 40.8 jit_solution(6549327456385121240)
XLA Ops:
  0.6 35.2 %attn_back.1 = (bf16[16,2048]{1,0:T(8,128)(2,1)}, bf16[48,2048]{1,0:T(8,128)(2,1)}, bf16[512,512]{1,0:T(8,128)(2,1)}) custom-call(bf16[128,2048]{1,0:T(8,128)(2,1)} %target_h.1, bf16[384,2048]{1,0:T(8,128)(2,1)} %source_h.1, bf16[128,2048]{1,0:T(8,128)(2,1)} %cot_h.1, f32[1,2048]{1,0:T(1,128)} %bitcast.2, f32[1,2048]{1,0:T(1,128)} %bitcast.3, ...), custom_call_target="tpu_custom_call" | custom-call | tf_op jit(solution)/shard_map/attn_back/pallas_call | solution.py:271
  35.9 1.5 %copy.15 = bf16[16,2048]{1,0:T(8,128)(2,1)} copy(bf16[16,2048]{1,0:T(8,128)(2,1)} %get-tuple-element.6) | data formatting | bytes 131072
  37.3 1.6 %copy.16 = bf16[48,2048]{1,0:T(8,128)(2,1)} copy(bf16[48,2048]{1,0:T(8,128)(2,1)} %get-tuple-element.7) | data formatting | bytes 393216
  39.0 1.9 %copy.17 = bf16[512,512]{1,0:T(8,128)(2,1)} copy(bf16[512,512]{1,0:T(8,128)(2,1)} %get-tuple-element.8) | data formatting | bytes 1048576

commit v2 on v1

--- a/solution.py
+++ b/solution.py
@@ -27,14 +27,14 @@
     return lax.rsqrt(jnp.mean(wide * wide, axis=1, keepdims=True) + NORM_EPS)
 
 
-def norm_into(src, gain, dst, block):
+def norm_into(src, gain, dst, block, base, count):
     def body(i, _):
-        rows = pl.ds(pl.multiple_of(i * block, block), block)
+        rows = pl.ds(pl.multiple_of(base + i * block, block), block)
         wide = src[rows, :].astype(F32)
         dst[rows, :] = (wide * inv_rms_of(wide) * gain[...]).astype(BF16)
         return 0
 
-    lax.fori_loop(0, src.shape[0] // block, body, 0)
+    lax.fori_loop(0, count // block, body, 0)
 
 
 def norm_back(wide, gain, upstream):
@@ -56,11 +56,11 @@
 
 def kernel(
     S, T,
-    target_h, source_h, cot_h, tgain, sgain, wq_h, wk_h, wv_h, wo_h,
-    gt_ref, gs_ref, go_ref,
-    target, source, cot, wq, wkv, wo, normed, kv, cotb, att, e_buf,
+    target_h, source_h, cot_h, tgain_h, sgain_h, wq_h, wk_h, wv_h, wo_h,
+    gt_out, gs_out, go_out,
+    target, source, cot, tgain, sgain, wq, wkv, wo, normed, kv, cotb, att, e_buf,
     kvg, kvg_in, red, red_in, red2, fin_in, pt, pt_in, ptr, ptr_in, stage,
-    load_sem, send, recv,
+    gt_ref, gs_ref, go_ref, load_sem, send, recv,
 ):
     Z = T // CORES
     me, t = lax.axis_index("sp"), lax.axis_index("tp")
@@ -76,8 +76,22 @@
     SR, RR = SG // T, TR // T
     inv_root = HEAD ** (-0.5)
 
-    def sp_peer(d):
-        return {"sp": lax.rem(me + d, S), "tp": t}
+    X = math.isqrt(S) if math.isqrt(S) ** 2 == S else S
+    Y = S // X
+    steps = sorted(
+        ((i // X, i % X) for i in range(S)), key=lambda yx: ((yx[0] > 0) + (yx[1] > 0), yx)
+    )
+    near = [d for d in range(1, S) if 0 in steps[d]]
+    far = [d for d in range(1, S) if 0 not in steps[d]]
+
+    def sp_place(d, way=1):
+        dy, dx = steps[d]
+        y = lax.rem(lax.div(me, X) + (dy if way > 0 else Y - dy), Y)
+        x = lax.rem(lax.rem(me, X) + (dx if way > 0 else X - dx), X)
+        return y * X + x
+
+    def sp_peer(d, way=1):
+        return {"sp": sp_place(d, way), "tp": t}
 
     def z_peer(d):
         return {"sp": me, "tp": lax.rem(z + d, Z) * CORES + c}
@@ -93,40 +107,45 @@
         sends.append(copy)
         return copy
 
-    loads = []
-    for i, (a, b) in enumerate(
-        (
-            (source_h, source), (wk_h, wkv.at[:, :HEAD]), (wv_h, wkv.at[:, HEAD:]),
-            (target_h, target), (wq_h, wq), (cot_h, cot), (wo_h, wo),
-        )
-    ):
-        copy = pltpu.make_async_copy(a, b, load_sem.at[i])
-        copy.start()
-        loads.append(copy)
+    mine = pl.ds(pl.multiple_of(c * half, half), half)
+    others = pl.ds(pl.multiple_of((1 - c) * half, half), half)
+    pairs = (
+        (source_h.at[mine], source.at[mine]), (wk_h, wkv.at[:, :HEAD]), (wv_h, wkv.at[:, HEAD:]),
+        (target_h, target), (wq_h, wq), (cot_h, cot), (wo_h, wo),
+        (sgain_h, sgain), (tgain_h, tgain), (source_h.at[others], source.at[others]),
+    )
+    loads = [pltpu.make_async_copy(a, b, load_sem.at[i]) for i, (a, b) in enumerate(pairs)]
+    for i in (7, 0, 1, 2):
+        loads[i].start()
 
     barrier = pltpu.get_barrier_semaphore()
     friends = [sibling] + [sp_peer(d) for d in range(1, S)] + [z_peer(d) for d in range(1, Z)]
     for who in friends:
         pl.semaphore_signal(barrier, inc=1, device_id=who, device_id_type=MESH)
 
+    loads[7].wait()
     loads[0].wait()
-    norm_into(source, sgain, normed, 32)
+    for i in (9, 3, 5, 8, 4, 6):
+        loads[i].start()
+    norm_into(source, sgain, normed, 32, c * half, half)
     loads[1].wait()
     loads[2].wait()
-    kv_own = dot(normed[...], wkv[...]).astype(BF16)
-    kv[0, 0] = kv_own[:half]
-    kv[0, 1] = kv_own[half:]
+    kv[0, c] = dot(normed[mine, :], wkv[...]).astype(BF16)
     pl.semaphore_wait(barrier, len(friends))
     kv_put = [None] + [put(kv.at[0, c], kv.at[d, c], 0, d, sp_peer(d)) for d in range(1, S)]
     loads[5].wait()
     cot_put = [None]
     for d in range(1, S):
-        columns = pl.ds(pl.multiple_of(lax.rem(me + d, S) * W, 128), W)
+        columns = pl.ds(pl.multiple_of(sp_place(d) * W, 128), W)
         rows = pl.ds(pl.multiple_of(c * thalf, thalf), thalf)
         cot_put.append(put(cot.at[rows, columns], cotb.at[d, c], 1, d, sp_peer(d)))
 
+    loads[9].wait()
+    norm_into(source, sgain, normed, 32, (1 - c) * half, half)
+    kv[0, 1 - c] = dot(normed[others, :], wkv[...]).astype(BF16)
+    loads[8].wait()
     loads[3].wait()
-    norm_into(target, tgain, normed, 32)
+    norm_into(target, tgain, normed, 32, 0, TR)
     loads[4].wait()
     query = dot(normed[:TR, :], wq[...]).astype(BF16)
     loads[6].wait()
@@ -157,7 +176,7 @@
     att_t = (out_t * inv_total).astype(BF16)
     att[0] = att_t
     delta = jnp.sum(att_t.astype(F32) * g_rows.astype(F32).T, axis=0, keepdims=True)
-    att_put = [None] + [put(att.at[0], att.at[d], 3, d, sp_peer(d)) for d in range(1, S)]
+    att_put = {d: put(att.at[0], att.at[d], 3, d, sp_peer(d)) for d in near}
 
     def spread(d, grads):
         if SR % 8:
@@ -171,12 +190,12 @@
         kvg_put[d].wait_recv()
         red[d] = (kvg[c, d].astype(F32) + kvg_in[d].astype(F32)).astype(BF16)
         if d:
-            return put(red.at[d], red_in.at[d], 5, d, sp_peer(S - d))
+            return put(red.at[d], red_in.at[d], 5, d, sp_peer(d, -1))
 
     kvg_put = {}
     red_put = {}
     gq_t = None
-    order = list(range(1, S)) + [0]
+    order = list(range(S - 1, -1, -1))
     for step, d in enumerate(order):
         k, v = pair(d)
         p = e_buf[d] * inv_total
@@ -190,6 +209,8 @@
         if step:
             red_put[order[step - 1]] = settle(order[step - 1])
 
+    for d in far:
+        att_put[d] = put(att.at[0], att.at[d], 3, d, sp_peer(d))
     gq_t = gq_t * inv_root
     gq = jnp.concatenate([gq_t[:, h * TR:(h + 1) * TR].T for h in range(H)], axis=1).astype(BF16)
     pulled = dot(gq, wq[...], NT)
@@ -232,19 +253,28 @@
         left = jnp.concatenate([a[:, h * TR:(h + 1) * TR] for a in att_all], axis=1)
         go_ref[h * HEAD:(h + 1) * HEAD, :] = dot(left, cot_rows).astype(BF16)
 
+    writes = [
+        pltpu.make_async_copy(a, b, load_sem.at[i])
+        for i, (a, b) in enumerate(((go_ref, go_out), (gt_ref, gt_out), (gs_ref, gs_out)))
+    ]
+    writes[0].start()
     up = ptr[z].astype(F32)
     for d in range(1, Z):
         ptr_put[d].wait_recv()
         up = up + ptr_in[d].astype(F32)
     gt_ref[...] = norm_back(own_rows(target, t, RR), tgain[...], up).astype(BF16)
+    writes[1].start()
     last = red2[z].astype(F32)
     for d in range(1, Z):
         fin_put[d].wait_recv()
         last = last + fin_in[d].astype(F32)
     up = dot(last.astype(BF16), wkv[...], NT)
     gs_ref[...] = norm_back(own_rows(source, t, SR), sgain[...], up).astype(BF16)
+    writes[2].start()
     for copy in sends:
         copy.wait_send()
+    for copy in writes:
+        copy.wait()
 
 
 def stage_rows(buf, rows):
@@ -265,20 +295,19 @@
     Z = T // CORES
     SR, RR, W = SG // T, TR // T, D // S
     N = max(S, Z)
-    hbm = pl.BlockSpec(memory_space=pl.ANY)
-    vm = pl.BlockSpec(memory_space=pltpu.VMEM)
+    hbm = pl.BlockSpec(memory_space=pltpu.HBM)
     V = pltpu.VMEM
-    return pl.pallas_call(
+    results = pl.pallas_call(
         functools.partial(kernel, S, T),
         out_shape=(
             jax.ShapeDtypeStruct((RR, D), BF16),
             jax.ShapeDtypeStruct((SR, D), BF16),
             jax.ShapeDtypeStruct((QW, W), BF16),
         ),
-        in_specs=[hbm, hbm, hbm, vm, vm, hbm, hbm, hbm, hbm],
-        out_specs=(vm, vm, vm),
+        in_specs=[hbm] * 9,
+        out_specs=(hbm, hbm, hbm),
         scratch_shapes=[
-            V((TR, D), BF16), V((SG, D), BF16), V((TR, D), BF16),
+            V((TR, D), BF16), V((SG, D), BF16), V((TR, D), BF16), V((1, D), F32), V((1, D), F32),
             V((D, QW), BF16), V((D, 2 * HEAD), BF16), V((QW, D), BF16),
             V((max(SG, TR), D), BF16),
             V((S, 2, SG // 2, 2 * HEAD), BF16), V((S, 2, TR // 2, W), BF16),
@@ -288,7 +317,8 @@
             V((Z, SR, 2 * HEAD), BF16), V((Z, SR, 2 * HEAD), BF16),
             V((CORES, Z, RR, D), BF16), V((Z, RR, D), BF16), V((Z, RR, D), BF16), V((Z, RR, D), BF16),
             V((SG, 2 * HEAD), F32),
-            pltpu.SemaphoreType.DMA((7,)),
+            V((RR, D), BF16), V((SR, D), BF16), V((QW, W), BF16),
+            pltpu.SemaphoreType.DMA((10,)),
             pltpu.SemaphoreType.DMA((10, N)),
             pltpu.SemaphoreType.DMA((10, N)),
         ],
@@ -300,6 +330,29 @@
         target, source, cotangent, target_gain.reshape(1, D), source_gain.reshape(1, D),
         w_query, w_key, w_value, w_out,
     )
+    return pl.pallas_call(
+        put_out,
+        out_shape=tuple(jax.ShapeDtypeStruct(r.shape, r.dtype) for r in results),
+        in_specs=[hbm, hbm, hbm],
+        out_specs=(hbm, hbm, hbm),
+        scratch_shapes=[V(r.shape, r.dtype) for r in results]
+        + [pltpu.SemaphoreType.DMA((3,)), pltpu.SemaphoreType.DMA((3,))],
+        compiler_params=pltpu.CompilerParams(vmem_limit_bytes=60 * 1024 * 1024),
+        name="put_out",
+    )(*results)
+
+
+def put_out(a, b, c, a_out, b_out, c_out, a_mid, b_mid, c_mid, in_sem, out_sem):
+    trios = ((a, a_mid, a_out), (b, b_mid, b_out), (c, c_mid, c_out))
+    ins = [pltpu.make_async_copy(x, y, in_sem.at[i]) for i, (x, y, _) in enumerate(trios)]
+    outs = [pltpu.make_async_copy(x, y, out_sem.at[i]) for i, (_, x, y) in enumerate(trios)]
+    for copy in ins:
+        copy.start()
+    for before, after in zip(ins, outs):
+        before.wait()
+        after.start()
+    for copy in outs:
+        copy.wait()
 
 
 def solution(mesh):

time: 41.1 us -> 34.9 us (0.85)
  local copies, waits for them, and re-layouts: 4.96 us -> 0 us
  Pallas kernels: 35.2 us -> 34 us
    unnamed x3 -> x0, local copies, waits for them, and re-layouts: 4.96 us -> none
    pallas_call x1, Pallas kernels: 35.2 us -> 32 us  [on_device(): pl.pallas_call(functools.partial(kernel, S, T), out_shape=(jax.ShapeDtype...]
    pallas_call x0 -> x1, Pallas kernels: none -> 2.02 us  [on_device(): pl.pallas_call(put_out, out_shape=tuple((jax.ShapeDtypeStruct(r.shape, r....]
where the time goes in v2:
time: 34.9 us; the launch traced here: 34.7 us
  Pallas kernels  34 us (97%)
  between operations  0.64 us (2%)
    pallas_call x1, Pallas kernels, on_device(): pl.pallas_call(functools.partial(kernel, S, T), out_shape=(jax.ShapeDtype...  32 us
    pallas_call x1, Pallas kernels, on_device(): pl.pallas_call(put_out, out_shape=tuple((jax.ShapeDtypeStruct(r.shape, r....  2.02 us

profile of v2, /device:TPU:0, one launch (start us, length us, event | category | flops | bytes accessed | tf_op | source)
XLA Modules:
  0.0 34.7 jit_solution(983048610215253377)
XLA Ops:
  0.6 32.0 %attn_back.1 = (bf16[16,2048]{1,0:T(8,128)(2,1)}, bf16[48,2048]{1,0:T(8,128)(2,1)}, bf16[512,512]{1,0:T(8,128)(2,1)}) custom-call(bf16[128,2048]{1,0:T(8,128)(2,1)} %target_h.1, bf16[384,2048]{1,0:T(8,128)(2,1)} %source_h.1, bf16[128,2048]{1,0:T(8,128)(2,1)} %cot_h.1, f32[1,2048]{1,0:T(1,128)} %bitcast.2, f32[1,2048]{1,0:T(1,128)} %bitcast.3, ...), custom_call_target="tpu_custom_call" | custom-call | tf_op jit(solution)/shard_map/attn_back/pallas_call | solution.py:300
  32.7 2.0 %put_out.1 = (bf16[16,2048]{1,0:T(8,128)(2,1)}, bf16[48,2048]{1,0:T(8,128)(2,1)}, bf16[512,512]{1,0:T(8,128)(2,1)}) custom-call(bf16[16,2048]{1,0:T(8,128)(2,1)} %get-tuple-element.6.a, bf16[48,2048]{1,0:T(8,128)(2,1)} %get-tuple-element.7.b, bf16[512,512]{1,0:T(8,128)(2,1)} %get-tuple-element.8.c), custom_call_target="tpu_custom_call" | custom-call | tf_op jit(solution)/shard_map/put_out/pallas_call | solution.py:333

commit v3 on v2

--- a/solution.py
+++ b/solution.py
@@ -37,9 +37,12 @@
     lax.fori_loop(0, count // block, body, 0)
 
 
-def norm_back(wide, gain, upstream):
+def unit_rows_of(wide):
     inv = inv_rms_of(wide)
-    unit = wide * inv
+    return inv, wide * inv
+
+
+def norm_back(inv, unit, gain, upstream):
     pulled = upstream * gain
     return inv * (pulled - unit * jnp.mean(pulled * unit, axis=1, keepdims=True))
 
@@ -58,7 +61,7 @@
     S, T,
     target_h, source_h, cot_h, tgain_h, sgain_h, wq_h, wk_h, wv_h, wo_h,
     gt_out, gs_out, go_out,
-    target, source, cot, tgain, sgain, wq, wkv, wo, normed, kv, cotb, att, e_buf,
+    target, source, cot, tgain, sgain, wq, wkv, wo, normed, kv, cotb, att, e_buf, pg_buf,
     kvg, kvg_in, red, red_in, red2, fin_in, pt, pt_in, ptr, ptr_in, stage,
     gt_ref, gs_ref, go_ref, load_sem, send, recv,
 ):
@@ -132,7 +135,7 @@
     loads[2].wait()
     kv[0, c] = dot(normed[mine, :], wkv[...]).astype(BF16)
     pl.semaphore_wait(barrier, len(friends))
-    kv_put = [None] + [put(kv.at[0, c], kv.at[d, c], 0, d, sp_peer(d)) for d in range(1, S)]
+    kv_put = {d: put(kv.at[0, c], kv.at[d, c], 0, d, sp_peer(d)) for d in far + near}
     loads[5].wait()
     cot_put = [None]
     for d in range(1, S):
@@ -161,17 +164,22 @@
         k, v = pair(d)
         e = jnp.exp2(dot(k, q_rows, NT) * (inv_root * math.log2(math.e)))
         e_buf[d] = e
+        pg_buf[d] = dot(v, g_rows, NT)
         return jnp.sum(e, axis=0, keepdims=True), dot(v, e.astype(BF16), TN)
 
     total, out_t = exponents(0)
-    kv_fwd = [None]
-    for d in range(1, S):
-        kv_put[d].wait_recv()
-        kv_fwd.append(put(kv.at[d, c], kv.at[d, c], 2, d, sibling))
-    for d in range(1, S):
-        kv_fwd[d].wait_recv()
-        more, out_more = exponents(d)
-        total, out_t = total + more, out_t + out_more
+    kv_fwd = {}
+    middle = len(near) // 2
+    arrivals = near[middle:] + far + near[:middle]
+    for step, d in enumerate(arrivals + [None]):
+        if d is not None:
+            kv_put[d].wait_recv()
+            kv_fwd[d] = put(kv.at[d, c], kv.at[d, c], 2, d, sibling)
+        if step:
+            before = arrivals[step - 1]
+            kv_fwd[before].wait_recv()
+            more, out_more = exponents(before)
+            total, out_t = total + more, out_t + out_more
     inv_total = 1.0 / total
     att_t = (out_t * inv_total).astype(BF16)
     att[0] = att_t
@@ -197,9 +205,9 @@
     gq_t = None
     order = list(range(S - 1, -1, -1))
     for step, d in enumerate(order):
-        k, v = pair(d)
+        k, _ = pair(d)
         p = e_buf[d] * inv_total
-        score_grad = (p * (dot(v, g_rows, NT) - delta)).astype(BF16)
+        score_grad = (p * (pg_buf[d] - delta)).astype(BF16)
         part = dot(k, score_grad, TN)
         gq_t = part if gq_t is None else gq_t + part
         k_grad = dot(score_grad, q_rows) * inv_root
@@ -258,18 +266,20 @@
         for i, (a, b) in enumerate(((go_ref, go_out), (gt_ref, gt_out), (gs_ref, gs_out)))
     ]
     writes[0].start()
+    target_inv, target_unit = unit_rows_of(own_rows(target, t, RR))
     up = ptr[z].astype(F32)
     for d in range(1, Z):
         ptr_put[d].wait_recv()
         up = up + ptr_in[d].astype(F32)
-    gt_ref[...] = norm_back(own_rows(target, t, RR), tgain[...], up).astype(BF16)
+    gt_ref[...] = norm_back(target_inv, target_unit, tgain[...], up).astype(BF16)
     writes[1].start()
+    source_inv, source_unit = unit_rows_of(own_rows(source, t, SR))
     last = red2[z].astype(F32)
     for d in range(1, Z):
         fin_put[d].wait_recv()
         last = last + fin_in[d].astype(F32)
     up = dot(last.astype(BF16), wkv[...], NT)
-    gs_ref[...] = norm_back(own_rows(source, t, SR), sgain[...], up).astype(BF16)
+    gs_ref[...] = norm_back(source_inv, source_unit, sgain[...], up).astype(BF16)
     writes[2].start()
     for copy in sends:
         copy.wait_send()
@@ -311,7 +321,7 @@
             V((D, QW), BF16), V((D, 2 * HEAD), BF16), V((QW, D), BF16),
             V((max(SG, TR), D), BF16),
             V((S, 2, SG // 2, 2 * HEAD), BF16), V((S, 2, TR // 2, W), BF16),
-            V((S, HEAD, R), BF16), V((S, SG, R), F32),
+            V((S, HEAD, R), BF16), V((S, SG, R), F32), V((S, SG, R), F32),
             V((CORES, S, Z, SR, 2 * HEAD), BF16), V((S, Z, SR, 2 * HEAD), BF16),
             V((S, Z, SR, 2 * HEAD), BF16), V((S, Z, SR, 2 * HEAD), BF16),
             V((Z, SR, 2 * HEAD), BF16), V((Z, SR, 2 * HEAD), BF16),

time: 34.9 us -> 35 us (level)
  no operation moved by 1% of the time
where the time goes in v3:
time: 35 us; the launch traced here: 34.8 us
  Pallas kernels  34.1 us (97%)
  between operations  0.64 us (2%)
    pallas_call x1, Pallas kernels, on_device(): pl.pallas_call(functools.partial(kernel, S, T), out_shape=(jax.ShapeDtype...  32.1 us
    pallas_call x1, Pallas kernels, on_device(): pl.pallas_call(put_out, out_shape=tuple((jax.ShapeDtypeStruct(r.shape, r....  2.02 us

profile of v3, /device:TPU:0, one launch (start us, length us, event | category | flops | bytes accessed | tf_op | source)
XLA Modules:
  0.0 34.8 jit_solution(12254084426302564465)
XLA Ops:
  0.6 32.1 %attn_back.1 = (bf16[16,2048]{1,0:T(8,128)(2,1)}, bf16[48,2048]{1,0:T(8,128)(2,1)}, bf16[512,512]{1,0:T(8,128)(2,1)}) custom-call(bf16[128,2048]{1,0:T(8,128)(2,1)} %target_h.1, bf16[384,2048]{1,0:T(8,128)(2,1)} %source_h.1, bf16[128,2048]{1,0:T(8,128)(2,1)} %cot_h.1, f32[1,2048]{1,0:T(1,128)} %bitcast.2, f32[1,2048]{1,0:T(1,128)} %bitcast.3, ...), custom_call_target="tpu_custom_call" | custom-call | tf_op jit(solution)/shard_map/attn_back/pallas_call | solution.py:310
  32.7 2.0 %put_out.1 = (bf16[16,2048]{1,0:T(8,128)(2,1)}, bf16[48,2048]{1,0:T(8,128)(2,1)}, bf16[512,512]{1,0:T(8,128)(2,1)}) custom-call(bf16[16,2048]{1,0:T(8,128)(2,1)} %get-tuple-element.6.a, bf16[48,2048]{1,0:T(8,128)(2,1)} %get-tuple-element.7.b, bf16[512,512]{1,0:T(8,128)(2,1)} %get-tuple-element.8.c), custom_call_target="tpu_custom_call" | custom-call | tf_op jit(solution)/shard_map/put_out/pallas_call | solution.py:343
